TPU v7x, 32 devices: a whole 2x2x4 slice. The times are simulated.
32 devices in a mesh: sp: 8 (over z, x), tp: 4 (over y, core).
Axes of the slice: x: 2, y: 2, z: 4, core: 2. Of those that a mesh axis runs over, the one named last changes fastest.
Arguments:
- queries: bfloat16 [2048, 1024], P('sp', 'tp'), may hold values from -6 to 6
- keys: bfloat16 [2048, 1024], P('sp', 'tp'), may hold values from -6 to 6
- values: bfloat16 [2048, 2048], P('sp', 'tp'), may hold values from -6 to 6
- gate_code: bfloat16 [2048, 32], P('sp'), may hold values from -5.5 to 5.5
- gate_up: bfloat16 [32, 1024], P(None, 'tp'), may hold values from -1 to 1
- gate_bias: float32 [1024], P('tp'), as said below
- gla_gain: float32 [256], replicated, may hold values from 0.1 to 1.9
- conv_input: bfloat16 [2048, 2048], P('sp', 'tp'), may hold values from -6 to 6
- conv_gate: bfloat16 [2048, 2048], P('sp', 'tp'), may hold values from -6 to 6
- conv_taps: float32 [3, 2048], P(None, 'tp'), may hold values from -3.5 to 3.5
- out_gla: bfloat16 [2048, 2048], P('tp', 'sp'), may hold values from -0.09375 to 0.09375
- out_conv: bfloat16 [2048, 2048], P('tp', 'sp'), may hold values from -0.09375 to 0.09375
Outputs:
- mixed: bfloat16 [2048, 2048], P(('sp', 'tp'))
Inputs may be any that keep to these rules, and one draw needn't show every extreme that they name: `gate_bias`: every bias is at least 1.5, so every decay per step lies strictly between 0 and 1.
All inputs are finite; a program needn't handle non-finite values.
Results may differ from a plain program's by a relative error of at most 0.028.
Values may be sent and summed in bfloat16 or wider, within the bound.
A program may use at most 64 MiB of HBM per device.

v0:
```python
import jax
import jax.numpy as jnp
from jax import lax
from jax.sharding import PartitionSpec as P

KEY_WIDTH = 128
HEAD_V = 256
SEGMENT_LENGTH = 64
softness_divisor = 16.0
epsilon = 1.0


def for_sending(x):
    return jax.tree.map(lambda a: a.astype(jnp.bfloat16) if a.dtype == jnp.float32 else a, x)


def from_behind(x, axis, by):
    count = lax.axis_size(axis)
    pairs = [(i, i + by) for i in range(count) if 0 <= i + by < count]
    return lax.ppermute(x, axis, pairs)


def chain(earlier, latter):
    return (earlier[0] * latter[0], latter[0][..., None] * earlier[1] + latter[1])


def per_device(
    queries,
    keys,
    values,
    gate_code,
    gate_up,
    gate_bias,
    gla_gain,
    conv_input,
    conv_gate,
    conv_taps,
    out_gla,
    out_conv,
):
    row_count = queries.shape[0]
    segment_count = row_count // SEGMENT_LENGTH
    head_count = queries.shape[1] // KEY_WIDTH
    gate_score = jnp.dot(gate_code, gate_up, preferred_element_type=jnp.float32) + gate_bias
    decay_logarithm = (jax.nn.log_sigmoid(gate_score) / softness_divisor).reshape(
        segment_count, SEGMENT_LENGTH, head_count, KEY_WIDTH
    )
    inside = jnp.cumsum(decay_logarithm, axis=1)
    seg_total = inside[:, -1]
    key_blocks = keys.reshape(segment_count, SEGMENT_LENGTH, head_count, KEY_WIDTH)
    scaled_keys = (key_blocks * jnp.exp(seg_total[:, None] - inside)).astype(jnp.bfloat16)
    value_blocks = values.reshape(segment_count, SEGMENT_LENGTH, head_count, HEAD_V)
    update = jnp.einsum(
        "nshk,nshv->nhkv", scaled_keys, value_blocks, preferred_element_type=jnp.float32
    )
    through, local_state = lax.associative_scan(chain, (jnp.exp(seg_total), update), axis=0)
    device_decay = through[-1]
    device_state = local_state[-1]
    columns = lax.all_to_all(
        device_state[None].astype(jnp.bfloat16), "sp", split_axis=3, concat_axis=0, tiled=True
    ).astype(jnp.float32)
    decays = lax.all_gather(device_decay[None], "sp", axis=0, tiled=True)
    running = lax.associative_scan(chain, (decays, columns), axis=0)[1]
    before = jnp.concatenate([jnp.zeros_like(running[:1]), running[:-1]], axis=0)
    incoming = lax.all_to_all(
        for_sending(before), "sp", split_axis=0, concat_axis=3, tiled=True
    ).astype(before.dtype)[0]
    states = local_state + through[..., None] * incoming[None]
    query_blocks = queries.reshape(segment_count, SEGMENT_LENGTH, head_count, KEY_WIDTH)
    readout = jnp.einsum(
        "nshk,nhkv->nshv",
        query_blocks,
        states.astype(jnp.bfloat16),
        preferred_element_type=jnp.float32,
    )
    norm_scale = lax.rsqrt(jnp.mean(readout * readout, axis=-1, keepdims=True) + epsilon)
    gla_mix = (
        (readout * norm_scale * gla_gain)
        .astype(jnp.bfloat16)
        .reshape(row_count, head_count * HEAD_V)
    )
    reach_rows = conv_taps.shape[0] - 1
    earlier_rows = from_behind(conv_input[row_count - reach_rows :], "sp", 1)
    extended = jnp.concatenate([earlier_rows, conv_input], axis=0)
    convolved = jnp.zeros(conv_input.shape, jnp.float32)
    for offset in range(reach_rows + 1):
        convolved = convolved + conv_taps[offset] * extended[offset : offset + row_count]
    conv_mix = (conv_gate * convolved).astype(jnp.bfloat16)
    wide_gla, wide_conv = (
        lax.all_gather(out_gla, "sp", axis=1, tiled=True),
        lax.all_gather(out_conv, "sp", axis=1, tiled=True),
    )
    summed = jnp.dot(gla_mix, wide_gla, preferred_element_type=jnp.float32)
    return lax.psum_scatter(
        (summed + jnp.dot(conv_mix, wide_conv, preferred_element_type=jnp.float32)).astype(
            jnp.bfloat16
        ),
        "tp",
        scatter_dimension=0,
        tiled=True,
    )


def solution(mesh):
    in_specs = (
        P("sp", "tp"),
        P("sp", "tp"),
        P("sp", "tp"),
        P("sp", None),
        P(None, "tp"),
        P("tp"),
        P(),
        P("sp", "tp"),
        P("sp", "tp"),
        P(None, "tp"),
        P("tp", "sp"),
        P("tp", "sp"),
    )
    out_specs = P(("sp", "tp"), None)
    return jax.shard_map(
        per_device, mesh=mesh, in_specs=in_specs, out_specs=out_specs, check_vma=False
    )
```

profile of v0, /device:TPU:0, one launch (start us, length us, event | category | flops | bytes accessed | tf_op | source)
XLA Modules:
  0.0 149.3 jit_solution(18421803840476476254)
XLA Ops:
  6.5 0.0 copy-start
  6.5 0.0 copy-start.3
  6.5 0.0 all-gather.3.cloned.1.call-start
  6.5 0.7 all-gather.3.cloned.1.call-update
  7.3 0.0 copy-done
  7.3 1.1 fusion.9
  8.3 0.1 reshape.57
  8.5 1.0 reshape.61
  9.5 0.0 copy-done.3
  9.5 0.1 reshape.58
  9.6 0.1 fusion.33
  9.8 0.2 multiply_convert_fusion.3
  10.0 0.3 fusion.11
  10.3 0.1 slice_add_fusion
  10.5 0.1 fusion.28
  10.6 0.1 fusion.27
  10.7 0.1 pad.49
  10.9 0.1 pad.50
  11.1 0.8 copy.32
  11.9 7.3 %all-to-all-start = ((bf16[1,2,128,256]{2,1,0,3:T(2,128)(2,1)}), bf16[1,2,128,256]{2,1,0,3:T(2,128)(2,1)S(1)}, u32[]{:S(2)}, u32[]{:S(2)}) async-start(bf16[1,2,128,256]{2,1,0,3:T(2,128)(2,1)} %copy.32), calls=%async_computation | async-start | bytes 262144 | tf_op jit(solution)/shard_map/all_to_all | solution.py:59
  19.1 0.0 all-gather.5.cloned.1.call-start
  19.2 0.7 all-gather.5.cloned.1.call-update
  19.9 0.0 copy-start.5
  20.0 0.0 copy-start.7
  20.0 21.3 %all_gather.9 = f32[8,2,128]{2,1,0:T(2,128)S(1)} all-gather(f32[1,2,128]{2,1,0:T(2,128)S(1)} %slice_add_fusion.5), channel_id=1, replica_groups=mesh['sp'=8,'tp'=4] {'sp'}, dimensions={0}, use_global_device_ids=true | all-gather | bytes 9216 | tf_op jit(solution)/shard_map/all_gather | solution.py:62
  41.4 0.6 copy.35
  42.0 0.0 all-to-all-done
  42.0 0.0 copy-done.5
  42.0 0.0 copy-done.7
  42.1 0.0 copy-start.1
  42.3 0.1 pad.138
  42.4 0.0 copy-start.4
  42.5 0.0 copy-start.6
  42.5 0.0 copy-start.8
  42.5 0.0 copy-start.9
  42.5 0.7 fusion.18
  43.2 0.1 pad.74
  43.4 0.7 concatenate.22.clone
  44.1 3.4 %all-to-all-start.1 = ((bf16[8,2,128,32]{2,3,1,0:T(8,128)(2,1)}), bf16[8,2,128,32]{2,3,1,0:T(8,128)(2,1)S(1)}, u32[]{:S(2)}, u32[]{:S(2)}) async-start(bf16[8,2,128,32]{2,3,1,0:T(8,128)(2,1)} %concatenate.22.clone), calls=%async_computation.1 | async-start | bytes 262144 | tf_op jit(solution)/shard_map/all_to_all | solution.py:65
  47.5 0.0 reduce-scatter.2.cloned.1.call-start
  47.5 0.0 copy-done.1
  47.5 3.8 %collective-permute-start = (bf16[2,512]{1,0:T(2,128)(2,1)S(1)}, bf16[2,512]{1,0:T(2,128)(2,1)S(1)}, u32[]{:S(2)}, u32[]{:S(2)}) collective-permute-start(bf16[2,512]{1,0:T(2,128)(2,1)S(1)} %slice.187), channel_id=1, source_target_pairs={{0,4},{4,8},{8,12},{12,16},{16,20},{20,24},{24,28},{1,5},{5,9},{9,... | collective-permute-start | bytes 6152 | tf_op jit(solution)/shard_map/ppermute | solution.py:20
  51.3 0.0 copy-done.6
  51.3 0.0 copy-done.8
  51.3 0.0 copy-done.4
  51.4 0.0 copy-start.10
  51.4 0.0 copy-done.9
  51.4 5.2 %all-to-all-done.1 = bf16[8,2,128,32]{2,3,1,0:T(8,128)(2,1)S(1)} async-done(((bf16[8,2,128,32]{2,3,1,0:T(8,128)(2,1)}), bf16[8,2,128,32]{2,3,1,0:T(8,128)(2,1)S(1)}, u32[]{:S(2)}, u32[]{:S(2)}) %all-to-all-start.1) | async-done | bytes 131104 | tf_op jit(solution)/shard_map/all_to_all | solution.py:65
  56.7 0.1 copy.40
  56.8 0.5 multiply_reduce_fusion
  57.3 0.0 copy-done.10
  57.3 0.1 multiply_convert_fusion.1
  57.4 0.3 copy.42
  57.7 8.6 %all-gather.3.cloned.1.call-done = bf16[512,2048]{1,0:T(8,128)(2,1)} async-done(((bf16[512,256]{1,0:T(8,128)(2,1)}), bf16[512,2048]{1,0:T(8,128)(2,1)}) %all-gather.3.cloned.1.call-update) | async-done | bytes 2097168 | tf_op jit(solution)/shard_map/all_gather | solution.py:90
  66.3 0.0 copy-start.2
  66.3 2.3 %fusion.34 = f32[256,2048]{1,0:T(8,128)S(1)} fusion(bf16[256,512]{1,0:T(8,128)(2,1)S(1)} %bitcast.43, bf16[512,2048]{1,0:T(8,128)(2,1)} %all-gather.3.cloned.1.call-done), kind=kOutput, calls=%fused_computation.81 | convolution fusion | flops 536870912 | bytes 4456448 | tf_op jit(solution)/shard_map/dot_general | solution.py:93
  68.7 0.0 collective-permute-done
  68.7 47.5 %all-gather.5.cloned.1.call-done = bf16[512,2048]{1,0:T(8,128)(2,1)} async-done(((bf16[512,256]{1,0:T(8,128)(2,1)}), bf16[512,2048]{1,0:T(8,128)(2,1)}) %all-gather.5.cloned.1.call-update) | async-done | bytes 2097168 | tf_op jit(solution)/shard_map/all_gather | solution.py:91
  116.2 0.0 copy-done.2
  116.2 3.4 %fusion = bf16[256,2048]{1,0:T(8,128)(2,1)} fusion(f32[256,2048]{1,0:T(8,128)S(1)} %fusion.34, bf16[512,2048]{1,0:T(8,128)(2,1)} %all-gather.5.cloned.1.call-done, bf16[256,512]{1,0:T(8,128)(2,1)S(1)} %copy-done.1, bf16[256,512]{1,0:T(8,128)(2,1)S(1)} %copy-done.2, bf16[2,512]{1,0:T(2,128)(2,1)S(1)} %collective-permute-done, f32[512]{0:T(512)S(1)} %bitcast.48, ...), kind=kOutput, calls=%fused_computation.1 | convolution fusion | flops 540147712 | bytes 5775360 | tf_op jit(solution)/shard_map/dot_general | solution.py:95
  119.6 0.0 reduce-scatter.2.cloned.1.call-update
  119.6 23.1 %reduce-scatter.2.cloned.1.call-done = bf16[64,2048]{1,0:T(8,128)(2,1)} async-done(((bf16[256,2048]{1,0:T(8,128)(2,1)}), bf16[64,2048]{1,0:T(8,128)(2,1)}) %reduce-scatter.2.cloned.1.call-update) | async-done | bytes 262160 | tf_op jit(solution)/shard_map/reduce_scatter | solution.py:94
  (42 shorter events, 0.7 us)
Async XLA Ops:
  6.5 0.7 copy-start
  6.5 3.0 %copy-start.3 = (bf16[256,512]{1,0:T(8,128)(2,1)S(1)}, bf16[256,512]{1,0:T(8,128)(2,1)}, u32[]{:S(2)}) copy-start(bf16[256,512]{1,0:T(8,128)(2,1)} %param.14) | copy-start | bytes 786436
  6.5 59.8 %all-gather.3.cloned.1.call-start = ((), (), s32[]{:S(2)}) async-start(), calls=%async_computation.3 | async-start | bytes 2359296 | tf_op jit(solution)/shard_map/all_gather | solution.py:90
  11.9 30.1 %all-to-all-start = ((bf16[1,2,128,256]{2,1,0,3:T(2,128)(2,1)}), bf16[1,2,128,256]{2,1,0,3:T(2,128)(2,1)S(1)}, u32[]{:S(2)}, u32[]{:S(2)}) async-start(bf16[1,2,128,256]{2,1,0,3:T(2,128)(2,1)} %copy.32), calls=%async_computation | async-start | bytes 262144 | tf_op jit(solution)/shard_map/all_to_all | solution.py:59
  19.1 97.1 %all-gather.5.cloned.1.call-start = ((), (), s32[]{:S(2)}) async-start(), calls=%async_computation.4 | async-start | bytes 2359296 | tf_op jit(solution)/shard_map/all_gather | solution.py:91
  19.9 22.1 %copy-start.5 = (f32[4,2,128]{2,1,0:T(2,128)}, f32[4,2,128]{2,1,0:T(2,128)S(1)}, u32[]{:S(2)}) copy-start(f32[4,2,128]{2,1,0:T(2,128)S(1)} %pad.53) | copy-start | bytes 12292
  20.0 22.0 %copy-start.7 = (f32[4,2,128]{2,1,0:T(2,128)}, f32[4,2,128]{2,1,0:T(2,128)S(1)}, u32[]{:S(2)}) copy-start(f32[4,2,128]{2,1,0:T(2,128)S(1)} %pad.54) | copy-start | bytes 12292
  42.1 5.4 %copy-start.1 = (bf16[256,512]{1,0:T(8,128)(2,1)S(1)}, bf16[256,512]{1,0:T(8,128)(2,1)}, u32[]{:S(2)}) copy-start(bf16[256,512]{1,0:T(8,128)(2,1)} %param.19) | copy-start | bytes 786436
  42.4 8.9 %copy-start.4 = (bf16[256,256]{1,0:T(8,128)(2,1)S(1)}, bf16[256,256]{1,0:T(8,128)(2,1)}, u32[]{:S(2)}) copy-start(bf16[256,256]{1,0:T(8,128)(2,1)} %param.12) | copy-start | bytes 393220
  42.5 8.9 %copy-start.6 = (f32[4,2,128]{2,1,0:T(2,128)S(1)}, f32[4,2,128]{2,1,0:T(2,128)}, u32[]{:S(2)}) copy-start(f32[4,2,128]{2,1,0:T(2,128)} %copy-done.5) | copy-start | bytes 12292
  42.5 8.9 %copy-start.8 = (f32[4,2,128]{2,1,0:T(2,128)S(1)}, f32[4,2,128]{2,1,0:T(2,128)}, u32[]{:S(2)}) copy-start(f32[4,2,128]{2,1,0:T(2,128)} %copy-done.7) | copy-start | bytes 12292
  42.5 8.9 %copy-start.9 = (f32[3,512]{1,0:T(4,128)S(1)}, f32[3,512]{1,0:T(4,128)}, u32[]{:S(2)}) copy-start(f32[3,512]{1,0:T(4,128)} %param.21) | copy-start | bytes 18436
  44.1 12.6 %all-to-all-start.1 = ((bf16[8,2,128,32]{2,3,1,0:T(8,128)(2,1)}), bf16[8,2,128,32]{2,3,1,0:T(8,128)(2,1)S(1)}, u32[]{:S(2)}, u32[]{:S(2)}) async-start(bf16[8,2,128,32]{2,3,1,0:T(8,128)(2,1)} %concatenate.22.clone), calls=%async_computation.1 | async-start | bytes 262144 | tf_op jit(solution)/shard_map/all_to_all | solution.py:65
  47.5 95.3 %reduce-scatter.2.cloned.1.call-start = ((), (), s32[]{:S(2)}) async-start(), calls=%async_computation.5 | async-start | bytes 1310720 | tf_op jit(solution)/shard_map/reduce_scatter | solution.py:94
  47.5 21.1 %collective-permute-start = (bf16[2,512]{1,0:T(2,128)(2,1)S(1)}, bf16[2,512]{1,0:T(2,128)(2,1)S(1)}, u32[]{:S(2)}, u32[]{:S(2)}) collective-permute-start(bf16[2,512]{1,0:T(2,128)(2,1)S(1)} %slice.187), channel_id=1, source_target_pairs={{0,4},{4,8},{8,12},{12,16},{16,20},{20,24},{24,28},{1,5},{5,9},{9,... | collective-permute-start | bytes 6152 | tf_op jit(solution)/shard_map/ppermute | solution.py:20
  51.4 5.9 %copy-start.10 = (f32[256]{0:T(256)S(1)}, f32[256]{0:T(256)}, u32[]{:S(2)}) copy-start(f32[256]{0:T(256)} %param.18) | copy-start | bytes 3076
  66.3 49.9 %copy-start.2 = (bf16[256,512]{1,0:T(8,128)(2,1)S(1)}, bf16[256,512]{1,0:T(8,128)(2,1)}, u32[]{:S(2)}) copy-start(bf16[256,512]{1,0:T(8,128)(2,1)} %param.20) | copy-start | bytes 786436
Sparse Core Ops, SparseCore 0:
  9.4 56.8 all-gather.2
  68.4 47.8 all-gather.4
  119.7 22.9 reduce-scatter.1
where the time goes:
time: 150 us; the launch traced here: 149 us
  waiting for transfers between devices  85.9 us (57%)
  blocking collectives  21.3 us (14%)
  starting transfers between devices  14.5 us (10%)
  between operations  13.7 us (9%)
  matrix products  7.61 us (5%)
  local copies, waits for them, and re-layouts  4.46 us (3%)
  other arithmetic  1.88 us (1%)
    all_gather x1, waiting for transfers between devices, per_device(): lax.all_gather(out_conv, 'sp', axis=1, tiled=True)  47.5 us
    reduce_scatter x1, waiting for transfers between devices, per_device(): lax.psum_scatter((summed + jnp.dot(conv_mix, wide_conv, preferred_element...  23.1 us
    all_gather x1, blocking collectives, per_device(): decays = lax.all_gather(device_decay[None], 'sp', axis=0, tiled=True)  21.3 us
    all_gather x1, waiting for transfers between devices, per_device(): lax.all_gather(out_gla, 'sp', axis=1, tiled=True)  8.57 us
    all_to_all x1, starting transfers between devices, per_device(): lax.all_to_all(device_state[None].astype(jnp.bfloat16), 'sp', split_axis=...  7.28 us
    all_to_all x1, waiting for transfers between devices, per_device(): lax.all_to_all(for_sending(before), 'sp', split_axis=0, concat_axis=3, ti...  5.2 us
    ppermute x1, starting transfers between devices, from_behind(): return lax.ppermute(x, axis, pairs)  3.77 us
    dot_general x1, matrix products, per_device(): jnp.dot(conv_mix, wide_conv, preferred_element_type=jnp.float32)  3.39 us
  transfers between devices with their start and end apart: 6, of which 4 were waited for; matrix products, arithmetic and copies ran while one was open for 7% of the time, Pallas kernels for 0%

commit v1 on v0

--- a/solution.py
+++ b/solution.py
@@ -8,6 +8,13 @@
 SEGMENT_LENGTH = 64
 softness_divisor = 16.0
 epsilon = 1.0
+
+
+def trade_parts(x, name, split, join):
+    size = lax.axis_size(name)
+    blocks = jnp.stack(jnp.split(x, size, axis=split), axis=0)
+    blocks = lax.all_to_all(blocks, name, split_axis=0, concat_axis=0)
+    return jnp.concatenate(blocks, axis=join)
 
 
 def for_sending(x):
@@ -62,9 +69,7 @@
     decays = lax.all_gather(device_decay[None], "sp", axis=0, tiled=True)
     running = lax.associative_scan(chain, (decays, columns), axis=0)[1]
     before = jnp.concatenate([jnp.zeros_like(running[:1]), running[:-1]], axis=0)
-    incoming = lax.all_to_all(
-        for_sending(before), "sp", split_axis=0, concat_axis=3, tiled=True
-    ).astype(before.dtype)[0]
+    incoming = trade_parts(for_sending(before), "sp", 0, 3).astype(before.dtype)[0]
     states = local_state + through[..., None] * incoming[None]
     query_blocks = queries.reshape(segment_count, SEGMENT_LENGTH, head_count, KEY_WIDTH)
     readout = jnp.einsum(

time: 150 us -> 152 us (1.013)
  local copies, waits for them, and re-layouts: 4.46 us -> 8.67 us
  waiting for transfers between devices: 85.9 us -> 83 us
    all_gather x1, waiting for transfers between devices: 8.57 us -> 4.37 us  [per_device(): lax.all_gather(out_gla, 'sp', axis=1, tiled=True)]
    unnamed x25 -> x26, local copies, waits for them, and re-layouts: 0.19 us -> 4.35 us
    all_gather x1, waiting for transfers between devices: 47.5 us -> 50.6 us  [per_device(): lax.all_gather(out_conv, 'sp', axis=1, tiled=True)]
    all_to_all x1, waiting for transfers between devices: 5.2 us -> 3.41 us  [trade_parts(): blocks = lax.all_to_all(blocks, name, split_axis=0, concat_axis=0)]
  transfers between devices with their start and end apart: 6 -> 6, of which waited for: 4 -> 4; matrix products, arithmetic and copies ran while one was open for 7% -> 10% of each run, Pallas kernels for 0% -> 0%
where the time goes in v1:
time: 152 us; the launch traced here: 151 us
  waiting for transfers between devices  83 us (55%)
  blocking collectives  21.3 us (14%)
  starting transfers between devices  14.5 us (10%)
  between operations  13.6 us (9%)
  local copies, waits for them, and re-layouts  8.67 us (6%)
  matrix products  7.63 us (5%)
  other arithmetic  2.55 us (2%)
    all_gather x1, waiting for transfers between devices, per_device(): lax.all_gather(out_conv, 'sp', axis=1, tiled=True)  50.6 us
    reduce_scatter x1, waiting for transfers between devices, per_device(): lax.psum_scatter((summed + jnp.dot(conv_mix, wide_conv, preferred_element...  23.1 us
    all_gather x1, blocking collectives, per_device(): decays = lax.all_gather(device_decay[None], 'sp', axis=0, tiled=True)  21.3 us
    all_to_all x1, starting transfers between devices, per_device(): lax.all_to_all(device_state[None].astype(jnp.bfloat16), 'sp', split_axis=...  7.28 us
    all_gather x1, waiting for transfers between devices, per_device(): lax.all_gather(out_gla, 'sp', axis=1, tiled=True)  4.37 us
    unnamed x26, local copies, waits for them, and re-layouts  4.35 us
    ppermute x1, starting transfers between devices, from_behind(): return lax.ppermute(x, axis, pairs)  3.77 us
    dot_general x1, matrix products, per_device(): jnp.dot(conv_mix, wide_conv, preferred_element_type=jnp.float32)  3.42 us
  transfers between devices with their start and end apart: 6, of which 4 were waited for; matrix products, arithmetic and copies ran while one was open for 10% of the time, Pallas kernels for 0%

profile of v1, /device:TPU:0, one launch (start us, length us, event | category | flops | bytes accessed | tf_op | source)
XLA Modules:
  0.0 151.2 jit_solution(9573472055956445038)
XLA Ops:
  6.5 0.0 copy-start
  6.5 0.0 copy-start.3
  6.5 0.0 all-gather.3.cloned.1.call-start
  6.5 0.7 all-gather.3.cloned.1.call-update
  7.3 0.0 copy-done
  7.3 1.1 fusion.9
  8.3 0.1 reshape.57
  8.5 1.0 reshape.61
  9.5 0.0 copy-done.3
  9.5 0.1 reshape.58
  9.6 0.1 fusion.33
  9.8 0.2 multiply_convert_fusion.3
  10.0 0.3 fusion.11
  10.3 0.1 slice_add_fusion
  10.5 0.1 fusion.28
  10.6 0.1 fusion.27
  10.7 0.1 pad.49
  10.9 0.1 pad.50
  11.1 0.8 copy.45
  11.9 7.3 %all-to-all-start = ((bf16[1,2,128,256]{2,1,0,3:T(2,128)(2,1)}), bf16[1,2,128,256]{2,1,0,3:T(2,128)(2,1)S(1)}, u32[]{:S(2)}, u32[]{:S(2)}) async-start(bf16[1,2,128,256]{2,1,0,3:T(2,128)(2,1)} %copy.45), calls=%async_computation | async-start | bytes 262144 | tf_op jit(solution)/shard_map/all_to_all | solution.py:66
  19.1 0.0 all-gather.5.cloned.1.call-start
  19.2 0.7 all-gather.5.cloned.1.call-update
  19.9 0.0 copy-start.5
  20.0 21.3 %all_gather.9 = f32[8,2,128]{2,1,0:T(2,128)S(1)} all-gather(f32[1,2,128]{2,1,0:T(2,128)S(1)} %slice_add_fusion.5), channel_id=1, replica_groups=mesh['sp'=8,'tp'=4] {'sp'}, dimensions={0}, use_global_device_ids=true | all-gather | bytes 9216 | tf_op jit(solution)/shard_map/all_gather | solution.py:69
  41.3 0.6 constant_dynamic-update-slice_fusion.7
  42.0 0.6 copy.48
  42.6 0.0 all-to-all-done
  42.6 0.0 copy-done.5
  42.6 0.0 copy-done.6
  42.7 0.0 copy-start.1
  42.9 0.1 pad.60
  43.0 0.0 copy-start.4
  43.0 0.7 fusion.18
  43.8 0.0 copy-start.7
  43.8 0.1 pad.59
  44.0 0.6 constant_dynamic-update-slice_fusion.6
  44.6 0.6 constant_dynamic-update-slice_fusion.5
  45.2 0.6 constant_dynamic-update-slice_fusion.4
  45.8 0.6 constant_dynamic-update-slice_fusion.3
  46.4 0.6 constant_dynamic-update-slice_fusion.2
  47.0 0.6 constant_dynamic-update-slice_fusion.1
  47.6 0.6 constant_dynamic-update-slice_fusion
  48.2 3.4 %all-to-all-start.1 = ((bf16[8,1,2,128,32]{3,4,2,1,0:T(8,128)(2,1)}), bf16[8,1,2,128,32]{3,4,2,1,0:T(8,128)(2,1)S(1)}, u32[]{:S(2)}, u32[]{:S(2)}) async-start(bf16[8,1,2,128,32]{3,4,2,1,0:T(8,128)(2,1)} %constant_dynamic-update-slice_fusion), calls=%async_computation.1 | async-start | bytes 262144 | tf_op jit(solution)/shard_map/all_to_all | solution.py:16
  51.6 0.0 reduce-scatter.2.cloned.1.call-start
  51.6 0.0 copy-done.1
  51.7 3.8 %collective-permute-start = (bf16[2,512]{1,0:T(2,128)(2,1)S(1)}, bf16[2,512]{1,0:T(2,128)(2,1)S(1)}, u32[]{:S(2)}, u32[]{:S(2)}) collective-permute-start(bf16[2,512]{1,0:T(2,128)(2,1)S(1)} %slice.198), channel_id=1, source_target_pairs={{0,4},{4,8},{8,12},{12,16},{16,20},{20,24},{24,28},{1,5},{5,9},{9,... | collective-permute-start | bytes 6152 | tf_op jit(solution)/shard_map/ppermute | solution.py:27
  55.4 0.7 add.120
  56.1 0.0 copy-done.4
  56.2 0.0 copy-done.7
  56.2 3.4 %all-to-all-done.1 = bf16[8,1,2,128,32]{3,4,2,1,0:T(8,128)(2,1)S(1)} async-done(((bf16[8,1,2,128,32]{3,4,2,1,0:T(8,128)(2,1)}), bf16[8,1,2,128,32]{3,4,2,1,0:T(8,128)(2,1)S(1)}, u32[]{:S(2)}, u32[]{:S(2)}) %all-to-all-start.1) | async-done | bytes 131104 | tf_op jit(solution)/shard_map/all_to_all | solution.py:16
  59.6 0.0 copy-start.8
  59.7 0.1 copy.57
  59.8 0.5 multiply_reduce_fusion
  60.3 0.0 copy-done.8
  60.3 0.1 multiply_convert_fusion.1
  60.5 0.3 copy.59
  60.8 4.4 %all-gather.3.cloned.1.call-done = bf16[512,2048]{1,0:T(8,128)(2,1)} async-done(((bf16[512,256]{1,0:T(8,128)(2,1)}), bf16[512,2048]{1,0:T(8,128)(2,1)}) %all-gather.3.cloned.1.call-update) | async-done | bytes 2097168 | tf_op jit(solution)/shard_map/all_gather | solution.py:95
  65.2 2.3 %fusion.34 = f32[256,2048]{1,0:T(8,128)S(1)} fusion(bf16[256,512]{1,0:T(8,128)(2,1)S(1)} %bitcast.78, bf16[512,2048]{1,0:T(8,128)(2,1)} %all-gather.3.cloned.1.call-done), kind=kOutput, calls=%fused_computation.96 | convolution fusion | flops 536870912 | bytes 4456448 | tf_op jit(solution)/shard_map/dot_general | solution.py:98
  67.5 0.0 collective-permute-done
  67.5 50.6 %all-gather.5.cloned.1.call-done = bf16[512,2048]{1,0:T(8,128)(2,1)} async-done(((bf16[512,256]{1,0:T(8,128)(2,1)}), bf16[512,2048]{1,0:T(8,128)(2,1)}) %all-gather.5.cloned.1.call-update) | async-done | bytes 2097168 | tf_op jit(solution)/shard_map/all_gather | solution.py:96
  118.1 0.0 copy-done.2
  118.2 3.4 %fusion = bf16[256,2048]{1,0:T(8,128)(2,1)} fusion(f32[256,2048]{1,0:T(8,128)S(1)} %fusion.34, bf16[512,2048]{1,0:T(8,128)(2,1)} %all-gather.5.cloned.1.call-done, bf16[256,512]{1,0:T(8,128)(2,1)S(1)} %copy-done.1, bf16[256,512]{1,0:T(8,128)(2,1)S(1)} %copy-done.2, bf16[2,512]{1,0:T(2,128)(2,1)S(1)} %collective-permute-done, f32[512]{0:T(512)S(1)} %bitcast.83, ...), kind=kOutput, calls=%fused_computation.1 | convolution fusion | flops 540147712 | bytes 5775360 | tf_op jit(solution)/shard_map/dot_general | solution.py:100
  121.6 0.0 reduce-scatter.2.cloned.1.call-update
  121.6 23.1 %reduce-scatter.2.cloned.1.call-done = bf16[64,2048]{1,0:T(8,128)(2,1)} async-done(((bf16[256,2048]{1,0:T(8,128)(2,1)}), bf16[64,2048]{1,0:T(8,128)(2,1)}) %reduce-scatter.2.cloned.1.call-update) | async-done | bytes 262160 | tf_op jit(solution)/shard_map/reduce_scatter | solution.py:99
  (43 shorter events, 0.7 us)
Async XLA Ops:
  6.5 0.7 copy-start
  6.5 3.0 %copy-start.3 = (bf16[256,512]{1,0:T(8,128)(2,1)S(1)}, bf16[256,512]{1,0:T(8,128)(2,1)}, u32[]{:S(2)}) copy-start(bf16[256,512]{1,0:T(8,128)(2,1)} %param.14) | copy-start | bytes 786436
  6.5 58.6 %all-gather.3.cloned.1.call-start = ((), (), s32[]{:S(2)}) async-start(), calls=%async_computation.3 | async-start | bytes 2359296 | tf_op jit(solution)/shard_map/all_gather | solution.py:95
  11.9 30.7 %all-to-all-start = ((bf16[1,2,128,256]{2,1,0,3:T(2,128)(2,1)}), bf16[1,2,128,256]{2,1,0,3:T(2,128)(2,1)S(1)}, u32[]{:S(2)}, u32[]{:S(2)}) async-start(bf16[1,2,128,256]{2,1,0,3:T(2,128)(2,1)} %copy.45), calls=%async_computation | async-start | bytes 262144 | tf_op jit(solution)/shard_map/all_to_all | solution.py:66
  19.1 99.0 %all-gather.5.cloned.1.call-start = ((), (), s32[]{:S(2)}) async-start(), calls=%async_computation.4 | async-start | bytes 2359296 | tf_op jit(solution)/shard_map/all_gather | solution.py:96
  19.9 22.6 %copy-start.5 = (f32[4,2,128]{2,1,0:T(2,128)}, f32[4,2,128]{2,1,0:T(2,128)S(1)}, u32[]{:S(2)}) copy-start(f32[4,2,128]{2,1,0:T(2,128)S(1)} %pad.53) | copy-start | bytes 12292
  20.0 22.6 %copy-start.6 = (f32[4,2,128]{2,1,0:T(2,128)}, f32[4,2,128]{2,1,0:T(2,128)S(1)}, u32[]{:S(2)}) copy-start(f32[4,2,128]{2,1,0:T(2,128)S(1)} %pad.54) | copy-start | bytes 12292
  42.7 9.0 %copy-start.1 = (bf16[256,512]{1,0:T(8,128)(2,1)S(1)}, bf16[256,512]{1,0:T(8,128)(2,1)}, u32[]{:S(2)}) copy-start(bf16[256,512]{1,0:T(8,128)(2,1)} %param.19) | copy-start | bytes 786436
  43.0 13.1 %copy-start.4 = (bf16[256,256]{1,0:T(8,128)(2,1)S(1)}, bf16[256,256]{1,0:T(8,128)(2,1)}, u32[]{:S(2)}) copy-start(bf16[256,256]{1,0:T(8,128)(2,1)} %param.12) | copy-start | bytes 393220
  43.8 12.4 %copy-start.7 = (f32[3,512]{1,0:T(4,128)S(1)}, f32[3,512]{1,0:T(4,128)}, u32[]{:S(2)}) copy-start(f32[3,512]{1,0:T(4,128)} %param.21) | copy-start | bytes 18436
  48.2 11.4 %all-to-all-start.1 = ((bf16[8,1,2,128,32]{3,4,2,1,0:T(8,128)(2,1)}), bf16[8,1,2,128,32]{3,4,2,1,0:T(8,128)(2,1)S(1)}, u32[]{:S(2)}, u32[]{:S(2)}) async-start(bf16[8,1,2,128,32]{3,4,2,1,0:T(8,128)(2,1)} %constant_dynamic-update-slice_fusion), calls=%async_computation.1 | async-start | bytes 262144 | tf_op jit(solution)/shard_map/all_to_all | solution.py:16
  51.6 93.1 %reduce-scatter.2.cloned.1.call-start = ((), (), s32[]{:S(2)}) async-start(), calls=%async_computation.5 | async-start | bytes 1310720 | tf_op jit(solution)/shard_map/reduce_scatter | solution.py:99
  51.7 15.8 %collective-permute-start = (bf16[2,512]{1,0:T(2,128)(2,1)S(1)}, bf16[2,512]{1,0:T(2,128)(2,1)S(1)}, u32[]{:S(2)}, u32[]{:S(2)}) collective-permute-start(bf16[2,512]{1,0:T(2,128)(2,1)S(1)} %slice.198), channel_id=1, source_target_pairs={{0,4},{4,8},{8,12},{12,16},{16,20},{20,24},{24,28},{1,5},{5,9},{9,... | collective-permute-start | bytes 6152 | tf_op jit(solution)/shard_map/ppermute | solution.py:27
  59.6 0.7 copy-start.8
  65.1 53.0 %copy-start.2 = (bf16[256,512]{1,0:T(8,128)(2,1)S(1)}, bf16[256,512]{1,0:T(8,128)(2,1)}, u32[]{:S(2)}) copy-start(bf16[256,512]{1,0:T(8,128)(2,1)} %param.20) | copy-start | bytes 786436
Sparse Core Ops, SparseCore 0:
  9.4 55.7 all-gather.2
  67.2 50.9 all-gather.4
  121.7 22.9 reduce-scatter.1
